TPU v7x, 32 devices: a whole 2x2x4 slice. The times are simulated.
32 devices in a mesh: ep: 16 (over z, y, x), tp: 2 (over core).
Axes of the slice: x: 2, y: 2, z: 4, core: 2. Of those that a mesh axis runs over, the one named last changes fastest.
Arguments:
- hidden: bfloat16 [352, 2048], P('ep'), may hold values from -6 to 6
- mixer_gain: bfloat16 [2048], replicated, may hold values from 0.099609375 to 1.8984375
- gate_proj: bfloat16 [2048, 1024], P(None, 'tp'), may hold values from -0.125 to 0.125
- value_proj: bfloat16 [2048, 1024], P(None, 'tp'), may hold values from -0.125 to 0.125
- write_proj: bfloat16 [2048, 512], P(None, 'tp'), may hold values from -0.125 to 0.125
- read_proj: bfloat16 [2048, 512], P(None, 'tp'), may hold values from -0.125 to 0.125
- step_proj: bfloat16 [2048, 16], replicated, may hold values from -0.125 to 0.125
- step_bias: float32 [16], replicated, may hold values from -3 to 0
- decay_log: float32 [16], replicated, may hold values from 0 to 2.77
- skip_gain: float32 [16], replicated, may hold values from 0.5 to 2
- value_taps: bfloat16 [4, 1024], replicated, may hold values from -3 to 3
- write_taps: bfloat16 [4, 512], replicated, may hold values from -3 to 3
- read_taps: bfloat16 [4, 512], replicated, may hold values from -3 to 3
- value_tail: bfloat16 [352, 3, 1024], P('ep', None, 'tp'), may hold values from -6 to 6
- write_tail: bfloat16 [352, 3, 512], P('ep', None, 'tp'), may hold values from -6 to 6
- read_tail: bfloat16 [352, 3, 512], P('ep', None, 'tp'), may hold values from -6 to 6
- scan_state: float32 [352, 16, 64, 128], P('ep', 'tp'), may hold values from -4 to 4
- group_gain: bfloat16 [1024], replicated, may hold values from 0.099609375 to 1.8984375
- out_proj: bfloat16 [1024, 2048], P('tp'), may hold values from -0.1875 to 0.1875
- ffn_gain: bfloat16 [2048], replicated, may hold values from 0.099609375 to 1.8984375
- group_router: bfloat16 [2048, 2], replicated, may hold values from -0.125 to 0.125
- expert_router: bfloat16 [2048, 16], replicated, may hold values from -0.125 to 0.125
- expert_choice: int32 [352, 3], P('ep'), may hold values from 0 to 15, as said below
- expert_gate: bfloat16 [16, 2048, 1024], P('ep', None, 'tp'), may hold values from -0.125 to 0.125
- expert_up: bfloat16 [16, 2048, 1024], P('ep', None, 'tp'), may hold values from -0.125 to 0.125
- expert_down: bfloat16 [16, 1024, 2048], P('ep', 'tp'), may hold values from -1 to 1
Outputs:
- layer_out: bfloat16 [352, 2048], P('ep', 'tp')
- new_state: float32 [352, 16, 64, 128], P('ep', 'tp')
Inputs may be any that keep to these rules, and one draw needn't show every extreme that they name: `expert_choice`: every row names 3 different experts of one group (numbers equal in // 8). The 22 rows of one device name no expert more than 6 times, and for every device some expert is named exactly 6 times.
All inputs are finite; a program needn't handle non-finite values.
Results may differ from a plain program's by a relative error of at most 0.017.
Values may be sent and summed in bfloat16 or wider, within the bound.
A program may use at most 128 MiB of HBM per device.

v0:
```python
import jax
import jax.numpy as jnp
from jax import lax
from jax.sharding import PartitionSpec as P

GROUP_SIZE = 8


EPSILON = 1e-06


def normed(values, gain):
    widened = values.astype(jnp.float32)
    scale = lax.rsqrt(jnp.mean(widened * widened, axis=-1, keepdims=True) + EPSILON)
    return widened * scale * gain.astype(jnp.float32)


def convolve(history, newest, kernel):
    summed = kernel[-1].astype(jnp.float32) * newest.astype(jnp.float32)
    for offset in range(history.shape[1]):
        summed = summed + kernel[offset].astype(jnp.float32) * history[:, offset].astype(
            jnp.float32
        )
    return jax.nn.silu(summed)


def project(left, right):
    return jnp.dot(left, right, preferred_element_type=jnp.float32)


def on_device(
    hidden,
    mixer_gain,
    gate_proj,
    value_proj,
    write_proj,
    read_proj,
    step_proj,
    step_bias,
    decay_log,
    skip_gain,
    value_taps,
    write_taps,
    read_taps,
    value_tail,
    write_tail,
    read_tail,
    scan_state,
    group_gain,
    out_proj,
    ffn_gain,
    group_router,
    expert_router,
    expert_choice,
    expert_gate,
    expert_up,
    expert_down,
):
    tp_count = lax.axis_size("tp")
    ep_count = lax.axis_size("ep")
    tp_index = lax.axis_index("tp")
    seq_rows = hidden.shape[0]
    mixer_in = normed(hidden, mixer_gain).astype(jnp.bfloat16)
    gate_new = project(mixer_in, gate_proj).astype(jnp.bfloat16)
    value_new = project(mixer_in, value_proj).astype(jnp.bfloat16)
    write_new = project(mixer_in, write_proj).astype(jnp.bfloat16)
    read_new = project(mixer_in, read_proj).astype(jnp.bfloat16)
    head_count = step_proj.shape[1] // tp_count
    head_start = tp_index * head_count
    step_local = lax.dynamic_slice_in_dim(step_proj, head_start, head_count, 1)
    bias_local = lax.dynamic_slice_in_dim(step_bias, head_start, head_count, 0)
    rate_local = jnp.exp(lax.dynamic_slice_in_dim(decay_log, head_start, head_count, 0))
    skip_local = lax.dynamic_slice_in_dim(skip_gain, head_start, head_count, 0)
    step_size = jax.nn.softplus(project(mixer_in, step_local) + bias_local)
    decay = jnp.exp(-step_size * rate_local)
    value_width = value_proj.shape[1]
    vector_width = write_proj.shape[1]
    value_conv = convolve(
        value_tail,
        value_new,
        lax.dynamic_slice_in_dim(value_taps, tp_index * value_width, value_width, 1),
    )
    write_conv = convolve(
        write_tail,
        write_new,
        lax.dynamic_slice_in_dim(write_taps, tp_index * vector_width, vector_width, 1),
    )
    read_conv = convolve(
        read_tail,
        read_new,
        lax.dynamic_slice_in_dim(read_taps, tp_index * vector_width, vector_width, 1),
    )
    state_size = scan_state.shape[3]
    group_count = vector_width // state_size
    per_group = head_count // group_count
    heads_value = value_conv.reshape(seq_rows, head_count, value_width // head_count)
    heads_write = jnp.repeat(
        write_conv.reshape(seq_rows, group_count, state_size), per_group, axis=1
    )
    heads_read = jnp.repeat(read_conv.reshape(seq_rows, group_count, state_size), per_group, axis=1)
    new_state = (
        decay[:, :, None, None] * scan_state
        + (step_size[:, :, None] * heads_value)[:, :, :, None] * heads_write[:, :, None, :]
    )
    mixed_heads = (
        jnp.einsum("thpn,thn->thp", new_state, heads_read, precision=lax.Precision.HIGHEST)
        + skip_local[None, :, None] * heads_value
    )
    gated = mixed_heads.reshape(seq_rows, value_width) * jax.nn.silu(gate_new.astype(jnp.float32))
    grouped = gated.reshape(seq_rows, group_count, value_width // group_count)
    grouped = grouped * lax.rsqrt(jnp.mean(grouped * grouped, axis=-1, keepdims=True) + EPSILON)
    gain_local = lax.dynamic_slice_in_dim(group_gain, tp_index * value_width, value_width, 0)
    mixed = (grouped.reshape(seq_rows, value_width) * gain_local.astype(jnp.float32)).astype(
        jnp.bfloat16
    )
    residual = hidden.astype(jnp.float32) + lax.psum(project(mixed, out_proj), "tp")
    ffn_in = normed(residual, ffn_gain).astype(jnp.bfloat16)
    group_weights = jnp.exp(project(ffn_in, group_router))
    group_prob = group_weights / jnp.sum(group_weights, axis=1, keepdims=True)
    group_of = expert_choice[:, 0] // GROUP_SIZE
    group_mask = jnp.arange(group_router.shape[1])[None, :] == group_of[:, None]
    chosen_prob = jnp.sum(jnp.where(group_mask, group_prob, 0.0), axis=1, keepdims=True)
    picked_exp = jnp.exp(jnp.take_along_axis(project(ffn_in, expert_router), expert_choice, axis=1))
    gates = chosen_prob * picked_exp / jnp.sum(picked_exp, axis=1, keepdims=True)
    experts_total = expert_router.shape[1]
    top_count = expert_choice.shape[1]
    capacity = top_count * ((seq_rows + experts_total - 1) // experts_total)
    flat_choice = expert_choice.reshape(-1)
    one_hot = (flat_choice[:, None] == jnp.arange(experts_total)[None, :]).astype(jnp.int32)
    earlier = jnp.cumsum(one_hot, axis=0) - one_hot
    position = jnp.sum(earlier * one_hot, axis=1)
    target = (flat_choice * capacity + position).reshape(seq_rows, top_count)
    routing = target[:, :, None] == jnp.arange(experts_total * capacity)[None, None, :]
    dispatch = jnp.any(routing, axis=1).T.astype(jnp.bfloat16)
    combine = jnp.sum(routing.astype(jnp.float32) * gates[:, :, None], axis=1)
    model_width = ffn_in.shape[1]
    half_width = model_width // tp_count
    own_columns = lax.dynamic_slice_in_dim(ffn_in, tp_index * half_width, half_width, 1)
    outgoing = (
        project(dispatch, own_columns).astype(jnp.bfloat16).reshape(ep_count, capacity, half_width)
    )
    arrived = lax.all_gather(
        lax.all_to_all(outgoing, "ep", split_axis=0, concat_axis=0, tiled=True),
        "tp",
        axis=2,
        tiled=True,
    )
    slot_total = arrived.shape[1]
    flat_rows = arrived.reshape(-1, model_width)
    activated = (
        jax.nn.silu(project(flat_rows, expert_gate[0])) * project(flat_rows, expert_up[0])
    ).astype(jnp.bfloat16)
    partial_value = project(activated, expert_down[0]).reshape(ep_count, slot_total, model_width)
    reduced = lax.psum_scatter(
        partial_value.astype(jnp.bfloat16), "tp", scatter_dimension=2, tiled=True
    )
    returned = lax.all_to_all(reduced, "ep", split_axis=0, concat_axis=0, tiled=True)
    expert_sum = jnp.dot(
        combine,
        returned.reshape(-1, half_width).astype(jnp.float32),
        precision=lax.Precision.HIGHEST,
    )
    residual_half = lax.dynamic_slice_in_dim(residual, tp_index * half_width, half_width, 1)
    layer_out = (residual_half + expert_sum).astype(jnp.bfloat16)
    return (layer_out, new_state)


def solution(mesh):
    placed = (
        P("ep", None),
        P(),
        P(None, "tp"),
        P(None, "tp"),
        P(None, "tp"),
        P(None, "tp"),
        P(),
        P(),
        P(),
        P(),
        P(),
        P(),
        P(),
        P("ep", None, "tp"),
        P("ep", None, "tp"),
        P("ep", None, "tp"),
        P("ep", "tp", None, None),
        P(),
        P("tp", None),
        P(),
        P(),
        P(),
        P("ep", None),
        P("ep", None, "tp"),
        P("ep", None, "tp"),
        P("ep", "tp", None),
    )
    return jax.shard_map(
        on_device,
        mesh=mesh,
        in_specs=placed,
        out_specs=(P("ep", "tp"), P("ep", "tp", None, None)),
        check_vma=False,
    )
```

profile of v0, /device:TPU:0, one launch (start us, length us, event | category | flops | bytes accessed | tf_op | source)
XLA Modules:
  0.0 118.6 jit_solution(12233197621004373188)
XLA Ops:
  7.2 0.9 dynamic_slice.31
  8.1 0.7 dynamic-slice_exponential_fusion
  8.8 0.7 dynamic_slice.36
  9.6 1.0 fusion.28
  10.6 0.7 convert_element_type.143
  11.3 1.1 multiply_exponential_fusion
  12.6 0.8 dynamic-slice_convert_fusion.10
  13.4 0.9 dynamic-slice_convert_fusion.3
  14.3 0.9 dynamic-slice_convert_fusion.6
  15.2 1.5 %divide_multiply_fusion.2 = f32[22,256]{1,0:T(8,128)S(1)} fusion(bf16[2048,256]{1,0:T(8,128)(2,1)} %param.30, bf16[22,3,256]{2,0,1:T(8,128)(2,1)} %param.40, f32[256]{0:T(256)S(1)} %bitcast.99, f32[256]{0:T(256)S(1)} %bitcast.101, f32[256]{0:T(256)S(1)} %bitcast.100, f32[256]{0:T(256)S(1)} %bitcast.102, bf16[22,2048]{1,0:T(8,128)(2,1)} %param.26, ...), kind=kOutput, calls=%fused_computation.69 | convolution fusion | flops 23339008 | bytes 1207384 | tf_op jit(solution)/shard_map/dot_general | solution.py:28
  16.8 1.5 %divide_multiply_fusion.1 = f32[22,256]{1,0:T(8,128)S(1)} fusion(bf16[2048,256]{1,0:T(8,128)(2,1)} %param.31, bf16[22,3,256]{2,0,1:T(8,128)(2,1)} %param.41, f32[256]{0:T(256)S(1)} %bitcast.98, f32[256]{0:T(256)S(1)} %bitcast.96, f32[256]{0:T(256)S(1)} %bitcast.97, f32[256]{0:T(256)S(1)} %bitcast.95, bf16[22,2048]{1,0:T(8,128)(2,1)} %param.26, ...), kind=kOutput, calls=%fused_computation.68 | convolution fusion | flops 23339008 | bytes 1207384 | tf_op jit(solution)/shard_map/dot_general | solution.py:28
  18.4 2.1 %divide_multiply_fusion = f32[22,512]{1,0:T(8,128)S(1)} fusion(bf16[2048,512]{1,0:T(8,128)(2,1)} %param.29, bf16[22,3,512]{2,0,1:T(8,128)(2,1)} %param.39, f32[512]{0:T(512)S(1)} %bitcast.94, f32[512]{0:T(512)S(1)} %bitcast.92, f32[512]{0:T(512)S(1)} %bitcast.93, f32[512]{0:T(512)S(1)} %bitcast.91, bf16[22,2048]{1,0:T(8,128)(2,1)S(1)} %copy-done.2, ...), kind=kOutput, calls=%fused_computation.51 | convolution fusion | flops 46497792 | bytes 2316376 | tf_op jit(solution)/shard_map/dot_general | solution.py:28
  20.7 4.6 %multiply_add_fusion = f32[22,8,64,128]{3,2,1,0:T(8,128)S(1)} fusion(f32[22,8,64,128]{3,2,1,0:T(8,128)} %param.42, f32[22,8,128]{2,1,0:T(8,128)S(1)} %bitcast.86, f32[22,8,64]{2,1,0:T(8,128)S(1)} %broadcast_multiply_fusion, f32[22,8]{1,0:T(8,128)S(1)} %copy.85), kind=kLoop, calls=%fused_computation.1 | loop fusion | flops 4325376 | bytes 11670208 | tf_op jit(solution)/shard_map/add | solution.py:102
  25.3 9.0 %fusion.54 = f32[22,8,1,64]{3,2,1,0:T(1,128)S(1)} fusion(f32[22,8,64,128]{3,2,1,0:T(8,128)S(1)} %multiply_add_fusion, f32[22,8,128,1]{2,3,1,0:T(1,128)S(1)} %bitcast.88), kind=kOutput, calls=%fused_computation.108 | convolution fusion | flops 17301504 | bytes 5902336 | tf_op jit(solution)/shard_map/thpn,thn->thp/dot_general | solution.py:106
  34.4 2.0 %fusion.52 = (f32[22,512]{1,0:T(8,128)S(1)}, f32[22,512]{1,0:T(8,128)S(1)}) fusion(f32[22,512]{1,0:T(8,128)S(1)} %reshape.132, bf16[2048,512]{1,0:T(8,128)(2,1)} %param.28, bf16[22,2048]{1,0:T(8,128)(2,1)S(1)} %copy-done.2, f32[2048]{0:T(1024)S(1)} %convert_element_type.143, f32[22]{0:T(128)S(1)} %add_rsqrt_fusion.2), kind=kOutput, calls=%fused_computation.106 | convolution fusion | flops 46407680 | bytes 2330712 | tf_op jit(solution)/shard_map/dot_general | solution.py:28
  36.8 2.7 %fusion.36 = f32[22,2048]{1,0:T(8,128)} fusion(bf16[512,2048]{1,0:T(8,128)(2,1)} %param.44, f32[22,512]{1,0:T(8,128)S(1)} %get-tuple-element.19, f32[22,512]{1,0:T(8,128)S(1)} %bitcast.90, f32[512]{0:T(512)S(1)} %dynamic-slice_convert_fusion.10), kind=kOutput, calls=%fused_computation.60 | convolution fusion | flops 46171136 | bytes 2369536 | tf_op jit(solution)/shard_map/dot_general | solution.py:28
  40.4 20.1 %all-reduce.2.cloned.1.call-done = f32[22,2048]{1,0:T(8,128)} async-done(((f32[22,2048]{1,0:T(8,128)}), f32[22,2048]{1,0:T(8,128)}) %all-reduce.2.cloned.1.call-update) | async-done | bytes 180240 | tf_op jit(solution)/shard_map/psum | solution.py:116
  60.4 1.1 multiply_reduce_fusion
  61.6 0.3 convolution_convert_fusion.1
  61.9 0.8 reshape.134
  62.6 6.8 %all-to-all-start = ((bf16[16,6,1024]{2,1,0:T(8,128)(2,1)}), bf16[16,6,1024]{2,1,0:T(8,128)(2,1)S(1)}, u32[]{:S(2)}, u32[]{:S(2)}) async-start(bf16[16,6,1024]{2,1,0:T(8,128)(2,1)} %reshape.134), calls=%async_computation | async-start | bytes 524288 | tf_op jit(solution)/shard_map/all_to_all | solution.py:143
  69.7 10.0 %all-to-all-done = bf16[16,6,1024]{2,1,0:T(8,128)(2,1)S(1)} async-done(((bf16[16,6,1024]{2,1,0:T(8,128)(2,1)}), bf16[16,6,1024]{2,1,0:T(8,128)(2,1)S(1)}, u32[]{:S(2)}, u32[]{:S(2)}) %all-to-all-start) | async-done | bytes 196640 | tf_op jit(solution)/shard_map/all_to_all | solution.py:143
  79.8 2.2 %all_gather.3 = bf16[16,6,2048]{2,1,0:T(8,128)(2,1)S(1)} all-gather(bf16[16,6,1024]{2,1,0:T(8,128)(2,1)S(1)} %all-to-all-done), channel_id=1, replica_groups=mesh['ep'=16,'tp'=2] {'tp'}, dimensions={2}, use_global_device_ids=true | all-gather | bytes 589824 | tf_op jit(solution)/shard_map/all_gather | solution.py:142
  82.1 2.2 %fusion.3 = f32[96,512]{1,0:T(8,128)S(1)} fusion(bf16[96,2048]{1,0:T(8,128)(2,1)S(1)} %reshape.135, bf16[1,2048,512]{2,1,0:T(8,128)(2,1)} %param.49), kind=kOutput, calls=%fused_computation.6 | convolution fusion | flops 201326592 | bytes 2686976 | tf_op jit(solution)/shard_map/dot_general | solution.py:28
  84.3 0.5 fusion.8
  84.8 1.2 %convolution_convert_fusion = bf16[16,6,2048]{2,0,1:T(8,128)(2,1)} fusion(bf16[1,512,2048]{2,1,0:T(8,128)(2,1)S(1)} %copy-done, bf16[16,6,512]{2,1,0:T(8,128)(2,1)S(1)} %dot_general.56), kind=kOutput, calls=%fused_computation.2 | convolution fusion | flops 201523200 | bytes 2588672 | tf_op jit(solution)/shard_map/dot_general | solution.py:28
  86.3 1.7 %gather_fusion = f32[66]{0:T(128)S(1)} fusion(f32[22,16]{0,1:T(8,128)S(1)} %fusion.55, s32[66]{0:T(128)S(1)} %reshape.158), kind=kCustom, calls=%fused_computation | custom fusion | bytes 1056 | tf_op jit(solution)/shard_map/jit(take_along_axis)/gather | solution.py:123
  88.4 3.6 %reduce-scatter.2.cloned.1.call-done = bf16[16,6,1024]{2,0,1:T(8,128)(2,1)} async-done(((bf16[16,6,2048]{2,0,1:T(8,128)(2,1)}), bf16[16,6,1024]{2,0,1:T(8,128)(2,1)}) %reduce-scatter.2.cloned.1.call-update) | async-done | bytes 196624 | tf_op jit(solution)/shard_map/reduce_scatter | solution.py:154
  92.0 1.7 %copy.92 = bf16[16,6,1024]{2,1,0:T(8,128)(2,1)} copy(bf16[16,6,1024]{2,0,1:T(8,128)(2,1)} %reduce-scatter.2.cloned.1.call-done) | data formatting | bytes 393216 | tf_op jit(solution)/shard_map/reduce_scatter | solution.py:154
  93.7 6.7 %all-to-all-start.1 = ((bf16[16,6,1024]{2,1,0:T(8,128)(2,1)}), bf16[16,6,1024]{2,1,0:T(8,128)(2,1)S(1)}, u32[]{:S(2)}, u32[]{:S(2)}) async-start(bf16[16,6,1024]{2,1,0:T(8,128)(2,1)} %copy.92), calls=%async_computation.2 | async-start | bytes 524288 | tf_op jit(solution)/shard_map/all_to_all | solution.py:157
  100.6 10.3 %all-to-all-done.1 = bf16[16,6,1024]{2,1,0:T(8,128)(2,1)S(1)} async-done(((bf16[16,6,1024]{2,1,0:T(8,128)(2,1)}), bf16[16,6,1024]{2,1,0:T(8,128)(2,1)S(1)}, u32[]{:S(2)}, u32[]{:S(2)}) %all-to-all-start.1) | async-done | bytes 196640 | tf_op jit(solution)/shard_map/all_to_all | solution.py:157
  110.9 0.8 fusion.11
  (64 shorter events, 3.0 us)
Async XLA Ops:
  7.2 77.7 %copy-start = (bf16[1,512,2048]{2,1,0:T(8,128)(2,1)S(1)}, bf16[1,512,2048]{2,1,0:T(8,128)(2,1)}, u32[]{:S(2)}) copy-start(bf16[1,512,2048]{2,1,0:T(8,128)(2,1)} %param.51) | copy-start | bytes 6291460
  7.2 11.2 %copy-start.2 = (bf16[22,2048]{1,0:T(8,128)(2,1)S(1)}, bf16[22,2048]{1,0:T(8,128)(2,1)}, u32[]{:S(2)}) copy-start(bf16[22,2048]{1,0:T(8,128)(2,1)} %param.26) | copy-start | bytes 270340
  7.2 53.3 %all-reduce.2.cloned.1.call-start = ((), (), s32[]{:S(2)}) async-start(), calls=%async_computation.3 | async-start | bytes 393216 | tf_op jit(solution)/shard_map/psum | solution.py:116
  25.2 9.1 %copy-start.1 = (f32[22,8,64,128]{3,2,1,0:T(8,128)}, f32[22,8,64,128]{3,2,1,0:T(8,128)S(1)}, u32[]{:S(2)}) copy-start(f32[22,8,64,128]{3,2,1,0:T(8,128)S(1)} %multiply_add_fusion) | copy-start | bytes 17301508
  36.5 3.0 %copy-start.4 = (s32[22,3]{0,1:T(4,128)S(1)}, s32[22,3]{0,1:T(4,128)}, u32[]{:S(2)}) copy-start(s32[22,3]{0,1:T(4,128)} %param.48) | copy-start | bytes 796
  36.5 3.8 %copy-start.5 = (bf16[2048]{0:T(1024)(128)(2,1)S(1)}, bf16[2048]{0:T(1024)(128)(2,1)}, u32[]{:S(2)}) copy-start(bf16[2048]{0:T(1024)(128)(2,1)} %param.45) | copy-start | bytes 12292
  62.6 17.1 %all-to-all-start = ((bf16[16,6,1024]{2,1,0:T(8,128)(2,1)}), bf16[16,6,1024]{2,1,0:T(8,128)(2,1)S(1)}, u32[]{:S(2)}, u32[]{:S(2)}) async-start(bf16[16,6,1024]{2,1,0:T(8,128)(2,1)} %reshape.134), calls=%async_computation | async-start | bytes 524288 | tf_op jit(solution)/shard_map/all_to_all | solution.py:143
  69.5 22.5 %reduce-scatter.2.cloned.1.call-start = ((), (), s32[]{:S(2)}) async-start(), calls=%async_computation.4 | async-start | bytes 589824 | tf_op jit(solution)/shard_map/reduce_scatter | solution.py:154
  82.1 2.2 %copy-start.6 = (bf16[1,2048,512]{2,1,0:T(8,128)(2,1)S(1)}, bf16[1,2048,512]{2,1,0:T(8,128)(2,1)}, u32[]{:S(2)}) copy-start(bf16[1,2048,512]{2,1,0:T(8,128)(2,1)} %param.50) | copy-start | bytes 6291460
  84.8 1.3 %copy-start.3 = (bf16[2048,16]{0,1:T(8,128)(2,1)S(1)}, bf16[2048,16]{0,1:T(8,128)(2,1)}, u32[]{:S(2)}) copy-start(bf16[2048,16]{0,1:T(8,128)(2,1)} %param.47) | copy-start | bytes 196612
  86.2 1.9 %copy-start.7 = (bf16[2048,2]{0,1:T(2,128)(2,1)S(1)}, bf16[2048,2]{0,1:T(2,128)(2,1)}, u32[]{:S(2)}) copy-start(bf16[2048,2]{0,1:T(2,128)(2,1)} %param.46) | copy-start | bytes 24580
  93.7 17.1 %all-to-all-start.1 = ((bf16[16,6,1024]{2,1,0:T(8,128)(2,1)}), bf16[16,6,1024]{2,1,0:T(8,128)(2,1)S(1)}, u32[]{:S(2)}, u32[]{:S(2)}) async-start(bf16[16,6,1024]{2,1,0:T(8,128)(2,1)} %copy.92), calls=%async_computation.2 | async-start | bytes 524288 | tf_op jit(solution)/shard_map/all_to_all | solution.py:157
Sparse Core Ops, SparseCore 0:
  39.6 20.7 all-reduce.1
  86.2 5.7 reduce-scatter.1
where the time goes:
time: 119 us
  waiting for transfers between devices  44 us (37%)
  matrix products  25.3 us (21%)
  between operations  14.4 us (12%)
  starting transfers between devices  13.6 us (11%)
  other arithmetic  10.9 us (9%)
  local copies, waits for them, and re-layouts  8.13 us (7%)
  blocking collectives  2.17 us (2%)
    psum x1, waiting for transfers between devices, on_device(): lax.psum(project(mixed, out_proj), 'tp')  20.1 us
    dot_general x12, matrix products, project(): return jnp.dot(left, right, preferred_element_type=jnp.float32)  15.4 us
    all_to_all x1, waiting for transfers between devices, on_device(): lax.all_to_all(reduced, 'ep', split_axis=0, concat_axis=0, tiled=True)  10.3 us
    all_to_all x1, waiting for transfers between devices, on_device(): lax.all_to_all(outgoing, 'ep', split_axis=0, concat_axis=0, tiled=True)  10 us
    dot_general x1, matrix products, on_device(): jnp.einsum('thpn,thn->thp', new_state, heads_read, precision=lax.Precisio...  9.02 us
    all_to_all x1, starting transfers between devices, on_device(): lax.all_to_all(outgoing, 'ep', split_axis=0, concat_axis=0, tiled=True)  6.83 us
    all_to_all x1, starting transfers between devices, on_device(): lax.all_to_all(reduced, 'ep', split_axis=0, concat_axis=0, tiled=True)  6.73 us
    add x1, other arithmetic, on_device(): decay[:, :, None, None] * scan_state  4.56 us
  transfers between devices with their start and end apart: 4, of which 4 were waited for; matrix products, arithmetic and copies ran while one was open for 3% of the time, Pallas kernels for 0%

commit v1 on v0

v1 whole, which is shorter than its diff:
```python
import functools

import jax
import jax.numpy as jnp
from jax import lax
from jax.experimental import pallas as pl
from jax.experimental.pallas import tpu as pltpu
from jax.sharding import PartitionSpec as P

GROUP_SIZE = 8
EPSILON = 1e-06
MESH = pl.DeviceIdType.MESH
F32 = jnp.float32
BF16 = jnp.bfloat16


def dot(left, right, left_dim=1, right_dim=0, **options):
    return lax.dot_general(
        left,
        right,
        (((left_dim,), (right_dim,)), ((), ())),
        preferred_element_type=F32,
        **options,
    )


def normed(widened, gain):
    scale = lax.rsqrt(jnp.mean(widened * widened, axis=-1, keepdims=True) + EPSILON)
    return widened * scale * gain


def mixer_kernel(
    names,
    *refs,
):
    count = len(names)
    hbm = dict(zip(names, refs[:count]))
    bias_ref, rate_ref, skip_ref = refs[count : count + 3]
    mixed_ref, state_out = refs[count + 3 : count + 5]
    vmem = dict(zip(names, refs[count + 5 : 2 * count + 5]))
    y_ref, load_sem, state_sem, out_sem = refs[2 * count + 5 :]
    tp = lax.axis_index("tp")
    rows, head_count, head_dim, state_size = state_out.shape
    copies = {}
    for number, name in enumerate(names):
        if name == "state":
            for t in range(rows):
                copies["state", t] = pltpu.make_async_copy(
                    hbm[name].at[t], vmem[name].at[t], state_sem.at[t]
                )
                copies["state", t].start()
        else:
            copies[name] = pltpu.make_async_copy(hbm[name], vmem[name], load_sem.at[number])
            copies[name].start()

    def get(name):
        copies[name].wait()
        return vmem[name]

    hidden = get("hidden")[...].astype(F32)
    mixer_in = normed(hidden, get("mixer_gain")[...]).astype(BF16)
    width = vmem["value_proj"].shape[1]
    lane_head = lax.broadcasted_iota(jnp.int32, (1, width), 1) // head_dim

    def spread(ref):
        total = jnp.zeros((1, width), F32)
        for h in range(head_count):
            total = jnp.where(lane_head == h, ref[tp * head_count + h], total)
        return total

    step_raw = dot(mixer_in, get("step_proj")[...], 1, 1)
    pick = (
        lax.broadcasted_iota(jnp.int32, (step_raw.shape[1], width), 0)
        == tp * head_count + lax.broadcasted_iota(jnp.int32, (step_raw.shape[1], width), 1) // head_dim
    ).astype(F32)
    step_in = dot(step_raw, pick, precision=lax.Precision.HIGHEST) + spread(bias_ref)
    step_size = jnp.maximum(step_in, 0.0) + jnp.log1p(jnp.exp(-jnp.abs(step_in)))
    decay = jnp.exp(-step_size * jnp.exp(spread(rate_ref)))

    def convolved(kind):
        taps = get(kind + "_taps")
        tail = get(kind + "_tail")
        newest = dot(mixer_in, get(kind + "_proj")[...]).astype(BF16).astype(F32)
        span = newest.shape[1]
        kernel = taps[:, pl.ds(pl.multiple_of(tp * span, 128), span)].astype(F32)
        last = kernel.shape[0] - 1
        summed = kernel[last : last + 1] * newest
        for j in range(last):
            summed = summed + kernel[j : j + 1] * tail[j].astype(F32)
        return summed * jax.nn.sigmoid(summed)

    write_conv = convolved("write")
    read_conv = convolved("read").astype(BF16)
    value_conv = convolved("value")
    drive = (step_size * value_conv).T
    groups = write_conv.shape[1] // state_size
    per_group = head_count // groups
    group_width = per_group * head_dim
    state = vmem["state"]
    outs = []
    for t in range(rows):
        copies["state", t].wait()
        for g in range(groups):
            write_row = write_conv[t : t + 1, g * state_size : (g + 1) * state_size]
            parts = []
            for h in range(g * per_group, (g + 1) * per_group):
                updated = (
                    decay[t : t + 1, h * head_dim : h * head_dim + 1] * state[t, h]
                    + drive[h * head_dim : (h + 1) * head_dim, t : t + 1] * write_row
                )
                state[t, h] = updated
                parts.append(updated.astype(BF16))
            read_row = read_conv[t : t + 1, g * state_size : (g + 1) * state_size]
            y_ref[t : t + 1, g * group_width : (g + 1) * group_width] = dot(
                read_row, jnp.concatenate(parts, axis=0), 1, 1
            )
        out = pltpu.make_async_copy(state.at[t], state_out.at[t], out_sem.at[t])
        out.start()
        outs.append(out)
    gate_new = dot(mixer_in, get("gate_proj")[...]).astype(BF16).astype(F32)
    gated = (y_ref[...] + spread(skip_ref) * value_conv) * (gate_new * jax.nn.sigmoid(gate_new))
    gain = get("group_gain")[:, pl.ds(pl.multiple_of(tp * width, 128), width)]
    for g in range(groups):
        lanes = slice(g * group_width, (g + 1) * group_width)
        mixed_ref[:, lanes] = normed(gated[:, lanes], gain[:, lanes]).astype(BF16)
    for out in outs:
        out.wait()


def expert_kernel(
    cap,
    mixed_ref,
    hidden_ref,
    gain_ref,
    group_ref,
    router_ref,
    choice_ref,
    out_hbm,
    gate_hbm,
    up_hbm,
    down_hbm,
    result_ref,
    out_ref,
    gate_ref,
    up_ref,
    down_ref,
    part_ref,
    part_in,
    ffn_ref,
    res_ref,
    outgoing,
    arrived,
    other,
    half_out,
    half_in,
    answer,
    returned,
    load_sem,
    local_sem,
    part_sem,
    send_sem,
    recv_sem,
    relay_sem,
    landed_sem,
    half_sem,
    back_sem,
    home_sem,
):
    ep_count = lax.axis_size("ep")
    me = lax.axis_index("ep")
    tp = lax.axis_index("tp")
    barrier = pltpu.get_barrier_semaphore()
    partner = (me, 1 - tp)

    def peer(step):
        return lax.rem(me + step, ep_count)

    def source(step):
        return lax.rem(me - step + ep_count, ep_count)

    def block(number):
        return pl.ds(pl.multiple_of(number * cap, cap), cap)

    pl.semaphore_signal(barrier, inc=1, device_id=partner, device_id_type=MESH)
    for step in range(1, ep_count):
        pl.semaphore_signal(barrier, inc=1, device_id=(peer(step), tp), device_id_type=MESH)
    loads = []
    pairs = ((out_hbm, out_ref), (gate_hbm.at[0], gate_ref), (up_hbm.at[0], up_ref), (down_hbm.at[0], down_ref))
    for number, (far, near) in enumerate(pairs):
        loads.append(pltpu.make_async_copy(far, near, load_sem.at[number]))
        loads[-1].start()

    slots = arrived.shape[0]
    tokens = hidden_ref.shape[0]
    row = lax.broadcasted_iota(jnp.int32, (slots, tokens), 0)
    choice = choice_ref[...]
    hit = choice[0:1] == row // cap
    for k in range(1, choice.shape[0]):
        hit = hit | (choice[k : k + 1] == row // cap)
    hit = hit.astype(F32)
    earlier = (
        lax.broadcasted_iota(jnp.int32, (tokens, tokens), 0)
        < lax.broadcasted_iota(jnp.int32, (tokens, tokens), 1)
    ).astype(BF16)
    position = dot(hit.astype(BF16), earlier)
    dispatch = jnp.where(position == (row % cap).astype(F32), hit, 0.0)

    loads[0].wait()
    part_ref[...] = dot(mixed_ref[...], out_ref[...])
    pl.semaphore_wait(barrier, ep_count)
    swap = pltpu.make_async_remote_copy(
        part_ref, part_in, part_sem.at[0], part_sem.at[1], device_id=partner, device_id_type=MESH
    )
    swap.start()
    swap.wait()
    residual = hidden_ref[...].astype(F32) + (part_ref[...] + part_in[...])
    res_ref[...] = residual
    ffn_in = normed(residual, gain_ref[...]).astype(BF16)
    ffn_ref[...] = ffn_in.astype(F32)
    half = arrived.shape[1]
    own = pl.ds(pl.multiple_of(tp * half, 128), half)
    not_own = pl.ds(pl.multiple_of((1 - tp) * half, 128), half)
    outgoing[...] = dot(dispatch.astype(BF16), ffn_ref[:, own].astype(BF16)).astype(BF16)
    sends = []
    for step in range(1, ep_count):
        sends.append(
            pltpu.make_async_remote_copy(
                outgoing.at[block(peer(step))],
                arrived.at[block(me)],
                send_sem.at[step],
                recv_sem.at[step],
                device_id=(peer(step), tp),
                device_id_type=MESH,
            )
        )
        sends[-1].start()
    keep = pltpu.make_async_copy(outgoing.at[block(me)], arrived.at[block(me)], local_sem.at[0])
    keep.start()
    relays = [
        pltpu.make_async_remote_copy(
            outgoing.at[block(me)],
            other.at[block(me)],
            relay_sem.at[0],
            landed_sem.at[0],
            device_id=partner,
            device_id_type=MESH,
        )
    ]
    relays[0].start()

    group_exp = jnp.exp(dot(group_ref[...], ffn_in, 1, 1))
    group_prob = group_exp / jnp.sum(group_exp, axis=0, keepdims=True)
    group_row = lax.broadcasted_iota(jnp.int32, group_prob.shape, 0)
    chosen = jnp.sum(
        jnp.where(group_row == choice[0:1] // GROUP_SIZE, group_prob, 0.0), axis=0, keepdims=True
    )
    logits = dot(router_ref[...], ffn_in, 1, 1)
    experts = logits.shape[0]
    widen = (
        lax.broadcasted_iota(jnp.int32, (slots, experts), 0) // cap
        == lax.broadcasted_iota(jnp.int32, (slots, experts), 1)
    ).astype(F32)
    wide = dot(widen, logits, precision=lax.Precision.HIGHEST)
    picked = jnp.where(hit > 0.0, jnp.exp(wide), 0.0)
    total = jnp.sum(jnp.where(row % cap == 0, picked, 0.0), axis=0, keepdims=True)
    combine = (jnp.where(dispatch > 0.0, picked, 0.0) * (chosen / total)).T
    combine_high = combine.astype(BF16)
    combine_low = (combine - combine_high.astype(F32)).astype(BF16)

    for step in range(1, ep_count):
        sends[step - 1].wait_recv()
        relays.append(
            pltpu.make_async_remote_copy(
                arrived.at[block(source(step))],
                other.at[block(source(step))],
                relay_sem.at[step],
                landed_sem.at[step],
                device_id=partner,
                device_id_type=MESH,
            )
        )
        relays[-1].start()
    keep.wait()
    loads[1].wait()
    loads[2].wait()
    mine = arrived[...]
    gate_part = dot(mine, gate_ref[own, :])
    up_part = dot(mine, up_ref[own, :])
    for relay in relays:
        relay.wait_recv()
    theirs = other[...]
    gate_full = gate_part + dot(theirs, gate_ref[not_own, :])
    up_full = up_part + dot(theirs, up_ref[not_own, :])
    activated = (gate_full * jax.nn.sigmoid(gate_full) * up_full).astype(BF16)
    loads[3].wait()
    half_out[...] = dot(activated, down_ref[:, not_own]).astype(BF16)
    trade = pltpu.make_async_remote_copy(
        half_out, half_in, half_sem.at[0], half_sem.at[1], device_id=partner, device_id_type=MESH
    )
    trade.start()
    kept = dot(activated, down_ref[:, own]).astype(BF16)
    trade.wait_recv()
    answer[...] = (kept.astype(F32) + half_in[...].astype(F32)).astype(BF16)
    backs = []
    for step in range(1, ep_count):
        backs.append(
            pltpu.make_async_remote_copy(
                answer.at[block(peer(step))],
                returned.at[block(me)],
                back_sem.at[step],
                home_sem.at[step],
                device_id=(peer(step), tp),
                device_id_type=MESH,
            )
        )
        backs[-1].start()
    keep_back = pltpu.make_async_copy(answer.at[block(me)], returned.at[block(me)], local_sem.at[1])
    keep_back.start()
    trade.wait_send()
    for send in sends:
        send.wait_send()
    for relay in relays:
        relay.wait_send()
    keep_back.wait()
    for back in backs:
        back.wait_recv()
    rows_back = returned[...]
    expert_sum = dot(combine_high, rows_back) + dot(combine_low, rows_back)
    result_ref[...] = (res_ref[:, own] + expert_sum).astype(BF16)
    for back in backs:
        back.wait_send()


def on_device(
    hidden,
    mixer_gain,
    gate_proj,
    value_proj,
    write_proj,
    read_proj,
    step_proj,
    step_bias,
    decay_log,
    skip_gain,
    value_taps,
    write_taps,
    read_taps,
    value_tail,
    write_tail,
    read_tail,
    scan_state,
    group_gain,
    out_proj,
    ffn_gain,
    group_router,
    expert_router,
    expert_choice,
    expert_gate,
    expert_up,
    expert_down,
):
    ep_count = lax.axis_size("ep")
    rows, model = hidden.shape
    width = value_proj.shape[1]
    anywhere = pl.BlockSpec(memory_space=pl.ANY)
    near = pl.BlockSpec(memory_space=pltpu.VMEM)
    scalars = pl.BlockSpec(memory_space=pltpu.SMEM)
    gains = jnp.concatenate([mixer_gain, ffn_gain, group_gain]).astype(F32)
    gains = gains.reshape(1, -1)
    flip = lambda array: jnp.transpose(array, (1, 0, 2))
    operands = {
        "hidden": hidden,
        "mixer_gain": gains[:, :model],
        "step_proj": step_proj.T,
        "write_taps": write_taps,
        "write_tail": flip(write_tail),
        "write_proj": write_proj,
        "read_taps": read_taps,
        "read_tail": flip(read_tail),
        "read_proj": read_proj,
        "value_taps": value_taps,
        "value_tail": flip(value_tail),
        "value_proj": value_proj,
        "state": scan_state,
        "gate_proj": gate_proj,
        "group_gain": gains[:, 2 * model :],
    }
    names = tuple(operands)
    dma = pltpu.SemaphoreType.DMA
    mixed, new_state = pl.pallas_call(
        functools.partial(mixer_kernel, names),
        out_shape=(
            jax.ShapeDtypeStruct((rows, width), BF16),
            jax.ShapeDtypeStruct(scan_state.shape, F32),
        ),
        in_specs=[anywhere] * len(names) + [scalars] * 3,
        out_specs=(near, anywhere),
        scratch_shapes=[pltpu.VMEM(operands[name].shape, operands[name].dtype) for name in names]
        + [pltpu.VMEM((rows, width), F32), dma((len(names),)), dma((rows,)), dma((rows,))],
        name="mixer",
    )(*operands.values(), step_bias, decay_log, skip_gain)

    experts = expert_router.shape[1]
    capacity = expert_choice.shape[1] * ((rows + experts - 1) // experts)
    cap = (capacity + 7) // 8 * 8
    slots = experts * cap
    half = model // lax.axis_size("tp")
    hidden_units = expert_gate.shape[2]
    buffer = pltpu.VMEM((slots, half), BF16)
    layer_out = pl.pallas_call(
        functools.partial(expert_kernel, cap),
        out_shape=jax.ShapeDtypeStruct((rows, half), BF16),
        in_specs=[near] * 6 + [anywhere] * 4,
        out_specs=near,
        scratch_shapes=[
            pltpu.VMEM(out_proj.shape, BF16),
            pltpu.VMEM((model, hidden_units), BF16),
            pltpu.VMEM((model, hidden_units), BF16),
            pltpu.VMEM((hidden_units, model), BF16),
            pltpu.VMEM((rows, model), F32),
            pltpu.VMEM((rows, model), F32),
            pltpu.VMEM((rows, model), F32),
            pltpu.VMEM((rows, model), F32),
            buffer,
            buffer,
            buffer,
            buffer,
            buffer,
            buffer,
            buffer,
            dma((4,)),
            dma((2,)),
            dma((2,)),
            dma((ep_count,)),
            dma((ep_count,)),
            dma((ep_count,)),
            dma((ep_count,)),
            dma((2,)),
            dma((ep_count,)),
            dma((ep_count,)),
        ],
        compiler_params=pltpu.CompilerParams(collective_id=0, has_side_effects=True),
        name="experts",
    )(
        mixed,
        hidden,
        gains[:, model : 2 * model],
        group_router.T,
        expert_router.T,
        expert_choice.T,
        out_proj,
        expert_gate,
        expert_up,
        expert_down,
    )
    return (layer_out, new_state)


def solution(mesh):
    placed = (
        P("ep", None),
        P(),
        P(None, "tp"),
        P(None, "tp"),
        P(None, "tp"),
        P(None, "tp"),
        P(),
        P(),
        P(),
        P(),
        P(),
        P(),
        P(),
        P("ep", None, "tp"),
        P("ep", None, "tp"),
        P("ep", None, "tp"),
        P("ep", "tp", None, None),
        P(),
        P("tp", None),
        P(),
        P(),
        P(),
        P("ep", None),
        P("ep", None, "tp"),
        P("ep", None, "tp"),
        P("ep", "tp", None),
    )
    return jax.shard_map(
        on_device,
        mesh=mesh,
        in_specs=placed,
        out_specs=(P("ep", "tp"), P("ep", "tp", None, None)),
        check_vma=False,
    )
```

time: 119 us -> 47.3 us (0.40)
  waiting for transfers between devices: 44 us -> 0 us
  Pallas kernels: 0 us -> 41 us
  matrix products: 25.3 us -> 0 us
  between operations: 14.4 us -> 0.65 us
  starting transfers between devices: 13.6 us -> 0 us
  other arithmetic: 10.9 us -> 1.22 us
  local copies, waits for them, and re-layouts: 8.13 us -> 4.08 us
  blocking collectives: 2.17 us -> 0 us
    pallas_call x0 -> x2, Pallas kernels: none -> 41 us  [the longest x1 28.1 us: on_device(): pl.pallas_call(functools.partial(expert_kernel, cap), out_shape=jax.Shape...]
    dot_general x14 -> x0, matrix products: 25.3 us -> none  [the longest x12 15.4 us: project(): return jnp.dot(left, right, preferred_element_type=jnp.float32)]
    all_to_all x2 -> x0, waiting for transfers between devices: 20.3 us -> none  [the longest x1 10.3 us: on_device(): lax.all_to_all(reduced, 'ep', split_axis=0, concat_axis=0, tiled=True)]
    psum x1 -> x0, waiting for transfers between devices: 20.1 us -> none  [on_device(): lax.psum(project(mixed, out_proj), 'tp')]
    all_to_all x2 -> x0, starting transfers between devices: 13.6 us -> none  [the longest x1 6.83 us: on_device(): lax.all_to_all(outgoing, 'ep', split_axis=0, concat_axis=0, tiled=True)]
    add x3 -> x0, other arithmetic: 4.64 us -> none  [the longest x1 4.56 us: on_device(): decay[:, :, None, None] * scan_state]
    reduce_scatter x1 -> x0, waiting for transfers between devices: 3.6 us -> none  [on_device(): lax.psum_scatter(partial_value.astype(jnp.bfloat16), 'tp', scatter_dimens...]
    reduce_sum x7 -> x0, other arithmetic: 2.5 us -> none  [the longest x2 2.09 us: normed(): jnp.mean(widened * widened, axis=-1, keepdims=True) + EPSILON]
  transfers between devices with their start and end apart: 4 -> 0, of which waited for: 4 -> 0; matrix products, arithmetic and copies ran while one was open for 3% -> 0% of each run, Pallas kernels for 0% -> 0%
where the time goes in v1:
time: 47.3 us; the launch traced here: 47 us
  Pallas kernels  41 us (87%)
  local copies, waits for them, and re-layouts  4.08 us (9%)
  other arithmetic  1.22 us (3%)
  between operations  0.65 us (1%)
    pallas_call x1, Pallas kernels, on_device(): pl.pallas_call(functools.partial(expert_kernel, cap), out_shape=jax.Shape...  28.1 us
    pallas_call x1, Pallas kernels, on_device(): pl.pallas_call(functools.partial(mixer_kernel, names), out_shape=(jax.Sha...  12.9 us
    concatenate x3, local copies, waits for them, and re-layouts, on_device(): gains = jnp.concatenate([mixer_gain, ffn_gain, group_gain]).astype(F32)  2.07 us
    unnamed x1, local copies, waits for them, and re-layouts  1.42 us

profile of v1, /device:TPU:0, one launch (start us, length us, event | category | flops | bytes accessed | tf_op | source)
XLA Modules:
  0.0 47.0 jit_solution(12319277107404324468)
XLA Ops:
  0.6 0.7 %concatenate.18 = bf16[1,1024]{1,0:T(2,128)(2,1)S(1)} reshape(bf16[1024]{0:T(1024)(128)(2,1)} %param.43) | data formatting | bytes 4096 | tf_op jit(solution)/shard_map/concatenate | solution.py:368
  1.3 0.7 %concatenate.16 = bf16[1,2048]{1,0:T(2,128)(2,1)S(1)} reshape(bf16[2048]{0:T(1024)(128)(2,1)} %param.27) | data formatting | bytes 8192 | tf_op jit(solution)/shard_map/concatenate | solution.py:368
  2.0 0.7 %concatenate.17 = bf16[1,2048]{1,0:T(2,128)(2,1)S(1)} reshape(bf16[2048]{0:T(1024)(128)(2,1)} %param.45) | data formatting | bytes 8192 | tf_op jit(solution)/shard_map/concatenate | solution.py:368
  2.7 0.6 %maximum_convert_fusion.2.refs_14_ = f32[1,1024]{1,0:T(1,128)} fusion(bf16[1,1024]{1,0:T(2,128)(2,1)S(1)} %concatenate.18, bf16[1,2048]{1,0:T(2,128)(2,1)S(1)} %concatenate.17, bf16[1,2048]{1,0:T(2,128)(2,1)S(1)} %concatenate.16), kind=kLoop, calls=%fused_computation.2 | loop fusion | flops 6144 | bytes 14336 | tf_op jit(solution)/shard_map/slice | solution.py:386
  3.3 0.6 %maximum_convert_fusion.1.gain_ref = f32[1,2048]{1,0:T(1,128)} fusion(bf16[1,1024]{1,0:T(2,128)(2,1)S(1)} %concatenate.18, bf16[1,2048]{1,0:T(2,128)(2,1)S(1)} %concatenate.17, bf16[1,2048]{1,0:T(2,128)(2,1)S(1)} %concatenate.16), kind=kLoop, calls=%fused_computation.1 | loop fusion | flops 12288 | bytes 18432 | tf_op jit(solution)/shard_map/slice | solution.py:447
  3.9 0.6 %slice.12.refs_1_ = f32[1,2048]{1,0:T(1,128)} slice(f32[1,5120]{1,0:T(1,128)S(1)} %maximum_convert_fusion), slice={[0:1], [0:2048]} | slice | bytes 16384 | tf_op jit(solution)/shard_map/slice | solution.py:373
  4.5 12.9 %mixer.1 = (bf16[22,512]{1,0:T(8,128)(2,1)}, f32[22,8,64,128]{3,2,1,0:T(8,128)}) custom-call(bf16[22,2048]{1,0:T(8,128)(2,1)} %hidden_ref.1, f32[1,2048]{1,0:T(1,128)} %slice.12.refs_1_, bf16[16,2048]{1,0:T(8,128)(2,1)} %bitcast.8, bf16[4,512]{1,0:T(4,128)(2,1)} %refs_3_.1, bf16[3,22,256]{2,1,0:T(8,128)(2,1)} %bitcast.10, bf16[2048,256]{1,0:T(8,128)(2,1)} %refs_5_.1, ...), custom_call_target="tpu_custom_call" | custom-call | tf_op jit(solution)/shard_map/mixer/pallas_call | solution.py:390
  17.4 28.1 %experts.1 = bf16[22,1024]{1,0:T(8,128)(2,1)} custom-call(bf16[22,512]{1,0:T(8,128)(2,1)} %get-tuple-element.4.mixed_ref, bf16[22,2048]{1,0:T(8,128)(2,1)} %hidden_ref.1, f32[1,2048]{1,0:T(1,128)} %maximum_convert_fusion.1.gain_ref, bf16[2,2048]{1,0:T(2,128)(2,1)} %bitcast.12, bf16[16,2048]{1,0:T(8,128)(2,1)} %bitcast.9, s32[3,22]{1,0:T(4,128)} %bitcast.13, ...), custom_call_target="tpu_custom_call" | custom-call | tf_op jit(solution)/shard_map/experts/pallas_call | solution.py:410
  45.6 1.4 %copy.29 = bf16[22,1024]{1,0:T(8,128)(2,1)} copy(bf16[22,1024]{1,0:T(8,128)(2,1)} %experts.1) | data formatting | bytes 90112
  (1 shorter events, 0.0 us)

commit v2 on v1

--- a/solution.py
+++ b/solution.py
@@ -9,6 +9,7 @@
 
 GROUP_SIZE = 8
 EPSILON = 1e-06
+CHUNKS = 4
 MESH = pl.DeviceIdType.MESH
 F32 = jnp.float32
 BF16 = jnp.bfloat16
@@ -22,6 +23,10 @@
         preferred_element_type=F32,
         **options,
     )
+
+
+def row_of(ref):
+    return ref[...].astype(F32).reshape(1, -1)
 
 
 def normed(widened, gain):
@@ -41,14 +46,16 @@
     y_ref, load_sem, state_sem, out_sem = refs[2 * count + 5 :]
     tp = lax.axis_index("tp")
     rows, head_count, head_dim, state_size = state_out.shape
+    edges = [rows * c // CHUNKS for c in range(CHUNKS + 1)]
     copies = {}
     for number, name in enumerate(names):
         if name == "state":
-            for t in range(rows):
-                copies["state", t] = pltpu.make_async_copy(
-                    hbm[name].at[t], vmem[name].at[t], state_sem.at[t]
+            for c in range(CHUNKS):
+                span = pl.ds(edges[c], edges[c + 1] - edges[c])
+                copies["state", c] = pltpu.make_async_copy(
+                    hbm[name].at[span], vmem[name].at[span], state_sem.at[c]
                 )
-                copies["state", t].start()
+                copies["state", c].start()
         else:
             copies[name] = pltpu.make_async_copy(hbm[name], vmem[name], load_sem.at[number])
             copies[name].start()
@@ -58,7 +65,7 @@
         return vmem[name]
 
     hidden = get("hidden")[...].astype(F32)
-    mixer_in = normed(hidden, get("mixer_gain")[...]).astype(BF16)
+    mixer_in = normed(hidden, row_of(get("mixer_gain"))).astype(BF16)
     width = vmem["value_proj"].shape[1]
     lane_head = lax.broadcasted_iota(jnp.int32, (1, width), 1) // head_dim
 
@@ -98,8 +105,7 @@
     group_width = per_group * head_dim
     state = vmem["state"]
     outs = []
-    for t in range(rows):
-        copies["state", t].wait()
+    def token(t):
         for g in range(groups):
             write_row = write_conv[t : t + 1, g * state_size : (g + 1) * state_size]
             parts = []
@@ -114,15 +120,22 @@
             y_ref[t : t + 1, g * group_width : (g + 1) * group_width] = dot(
                 read_row, jnp.concatenate(parts, axis=0), 1, 1
             )
-        out = pltpu.make_async_copy(state.at[t], state_out.at[t], out_sem.at[t])
-        out.start()
-        outs.append(out)
+
     gate_new = dot(mixer_in, get("gate_proj")[...]).astype(BF16).astype(F32)
-    gated = (y_ref[...] + spread(skip_ref) * value_conv) * (gate_new * jax.nn.sigmoid(gate_new))
-    gain = get("group_gain")[:, pl.ds(pl.multiple_of(tp * width, 128), width)]
+    gate_new = gate_new * jax.nn.sigmoid(gate_new)
+    gain = get("group_gain")
+    for c in range(CHUNKS):
+        copies["state", c].wait()
+        for t in range(edges[c], edges[c + 1]):
+            token(t)
+        span = pl.ds(edges[c], edges[c + 1] - edges[c])
+        outs.append(pltpu.make_async_copy(state.at[span], state_out.at[span], out_sem.at[c]))
+        outs[-1].start()
+    gain_row = gain[pl.ds(pl.multiple_of(tp * width, width), width)].astype(F32).reshape(1, width)
+    gated = (y_ref[...] + spread(skip_ref) * value_conv) * gate_new
     for g in range(groups):
         lanes = slice(g * group_width, (g + 1) * group_width)
-        mixed_ref[:, lanes] = normed(gated[:, lanes], gain[:, lanes]).astype(BF16)
+        mixed_ref[:, lanes] = normed(gated[:, lanes], gain_row[:, lanes]).astype(BF16)
     for out in outs:
         out.wait()
 
@@ -215,15 +228,16 @@
     swap.wait()
     residual = hidden_ref[...].astype(F32) + (part_ref[...] + part_in[...])
     res_ref[...] = residual
-    ffn_in = normed(residual, gain_ref[...]).astype(BF16)
+    ffn_in = normed(residual, row_of(gain_ref)).astype(BF16)
     ffn_ref[...] = ffn_in.astype(F32)
     half = arrived.shape[1]
     own = pl.ds(pl.multiple_of(tp * half, 128), half)
     not_own = pl.ds(pl.multiple_of((1 - tp) * half, 128), half)
     outgoing[...] = dot(dispatch.astype(BF16), ffn_ref[:, own].astype(BF16)).astype(BF16)
-    sends = []
-    for step in range(1, ep_count):
-        sends.append(
+    sends = {}
+    steps = sorted(range(1, ep_count), key=lambda step: abs(2 * step - ep_count))
+    for step in steps:
+        sends[step] = (
             pltpu.make_async_remote_copy(
                 outgoing.at[block(peer(step))],
                 arrived.at[block(me)],
@@ -233,7 +247,7 @@
                 device_id_type=MESH,
             )
         )
-        sends[-1].start()
+        sends[step].start()
     keep = pltpu.make_async_copy(outgoing.at[block(me)], arrived.at[block(me)], local_sem.at[0])
     keep.start()
     relays = [
@@ -267,8 +281,8 @@
     combine_high = combine.astype(BF16)
     combine_low = (combine - combine_high.astype(F32)).astype(BF16)
 
-    for step in range(1, ep_count):
-        sends[step - 1].wait_recv()
+    for step in reversed(steps):
+        sends[step].wait_recv()
         relays.append(
             pltpu.make_async_remote_copy(
                 arrived.at[block(source(step))],
@@ -302,7 +316,7 @@
     trade.wait_recv()
     answer[...] = (kept.astype(F32) + half_in[...].astype(F32)).astype(BF16)
     backs = []
-    for step in range(1, ep_count):
+    for step in steps:
         backs.append(
             pltpu.make_async_remote_copy(
                 answer.at[block(peer(step))],
@@ -317,7 +331,7 @@
     keep_back = pltpu.make_async_copy(answer.at[block(me)], returned.at[block(me)], local_sem.at[1])
     keep_back.start()
     trade.wait_send()
-    for send in sends:
+    for send in sends.values():
         send.wait_send()
     for relay in relays:
         relay.wait_send()
@@ -365,12 +379,10 @@
     anywhere = pl.BlockSpec(memory_space=pl.ANY)
     near = pl.BlockSpec(memory_space=pltpu.VMEM)
     scalars = pl.BlockSpec(memory_space=pltpu.SMEM)
-    gains = jnp.concatenate([mixer_gain, ffn_gain, group_gain]).astype(F32)
-    gains = gains.reshape(1, -1)
     flip = lambda array: jnp.transpose(array, (1, 0, 2))
     operands = {
         "hidden": hidden,
-        "mixer_gain": gains[:, :model],
+        "mixer_gain": mixer_gain,
         "step_proj": step_proj.T,
         "write_taps": write_taps,
         "write_tail": flip(write_tail),
@@ -381,9 +393,9 @@
         "value_taps": value_taps,
         "value_tail": flip(value_tail),
         "value_proj": value_proj,
+        "gate_proj": gate_proj,
         "state": scan_state,
-        "gate_proj": gate_proj,
-        "group_gain": gains[:, 2 * model :],
+        "group_gain": group_gain,
     }
     names = tuple(operands)
     dma = pltpu.SemaphoreType.DMA
@@ -396,7 +408,7 @@
         in_specs=[anywhere] * len(names) + [scalars] * 3,
         out_specs=(near, anywhere),
         scratch_shapes=[pltpu.VMEM(operands[name].shape, operands[name].dtype) for name in names]
-        + [pltpu.VMEM((rows, width), F32), dma((len(names),)), dma((rows,)), dma((rows,))],
+        + [pltpu.VMEM((rows, width), F32), dma((len(names),)), dma((CHUNKS,)), dma((CHUNKS,))],
         name="mixer",
     )(*operands.values(), step_bias, decay_log, skip_gain)
 
@@ -444,7 +456,7 @@
     )(
         mixed,
         hidden,
-        gains[:, model : 2 * model],
+        ffn_gain,
         group_router.T,
         expert_router.T,
         expert_choice.T,

time: 47.3 us -> 42.3 us (0.89)
  local copies, waits for them, and re-layouts: 4.08 us -> 1.42 us
  other arithmetic: 1.22 us -> 0 us
  Pallas kernels: 41 us -> 40 us
    pallas_call x1, Pallas kernels: 12.9 us -> 9.54 us  [on_device(): pl.pallas_call(functools.partial(mixer_kernel, names), out_shape=(jax.Sha...]
    pallas_call x1, Pallas kernels: 28.1 us -> 30.5 us  [on_device(): pl.pallas_call(functools.partial(expert_kernel, cap), out_shape=jax.Shape...]
    concatenate x3 -> x0, local copies, waits for them, and re-layouts: 2.07 us -> none  [on_device(): gains = jnp.concatenate([mixer_gain, ffn_gain, group_gain]).astype(F32)]
    slice x2 -> x0, other arithmetic: 1.2 us -> none  [the longest x1 0.6 us: on_device(): gains[:, model:2 * model]]
    slice x1 -> x0, local copies, waits for them, and re-layouts: 0.59 us -> none  [on_device(): gains[:, :model]]
where the time goes in v2:
time: 42.3 us; the launch traced here: 42.1 us
  Pallas kernels  40 us (95%)
  local copies, waits for them, and re-layouts  1.42 us (3%)
  between operations  0.65 us (2%)
    pallas_call x1, Pallas kernels, on_device(): pl.pallas_call(functools.partial(expert_kernel, cap), out_shape=jax.Shape...  30.5 us
    pallas_call x1, Pallas kernels, on_device(): pl.pallas_call(functools.partial(mixer_kernel, names), out_shape=(jax.Sha...  9.54 us
    unnamed x1, local copies, waits for them, and re-layouts  1.42 us

profile of v2, /device:TPU:0, one launch (start us, length us, event | category | flops | bytes accessed | tf_op | source)
XLA Modules:
  0.0 42.1 jit_solution(17134428639197809492)
XLA Ops:
  0.6 9.5 %mixer.1 = (bf16[22,512]{1,0:T(8,128)(2,1)}, f32[22,8,64,128]{3,2,1,0:T(8,128)}) custom-call(bf16[22,2048]{1,0:T(8,128)(2,1)} %hidden_ref.1, bf16[2048]{0:T(1024)(128)(2,1)} %refs_1_.1, bf16[16,2048]{1,0:T(8,128)(2,1)} %bitcast.9, bf16[4,512]{1,0:T(4,128)(2,1)} %refs_3_.1, bf16[3,22,256]{2,1,0:T(8,128)(2,1)} %bitcast.10, bf16[2048,256]{1,0:T(8,128)(2,1)} %refs_5_.1, ...), custom_call_target="tpu_custom_call" | custom-call | tf_op jit(solution)/shard_map/mixer/pallas_call | solution.py:402
  10.2 30.5 %experts.1 = bf16[22,1024]{1,0:T(8,128)(2,1)} custom-call(bf16[22,512]{1,0:T(8,128)(2,1)} %get-tuple-element.4.mixed_ref, bf16[22,2048]{1,0:T(8,128)(2,1)} %hidden_ref.1, bf16[2048]{0:T(1024)(128)(2,1)} %gain_ref.1, bf16[2,2048]{1,0:T(2,128)(2,1)} %bitcast.12, bf16[16,2048]{1,0:T(8,128)(2,1)} %bitcast.8, s32[3,22]{1,0:T(4,128)} %bitcast.13, ...), custom_call_target="tpu_custom_call" | custom-call | tf_op jit(solution)/shard_map/experts/pallas_call | solution.py:422
  40.7 1.4 %copy.29 = bf16[22,1024]{1,0:T(8,128)(2,1)} copy(bf16[22,1024]{1,0:T(8,128)(2,1)} %experts.1) | data formatting | bytes 90112

commit v3 on v2

--- a/solution.py
+++ b/solution.py
@@ -235,7 +235,7 @@
     not_own = pl.ds(pl.multiple_of((1 - tp) * half, 128), half)
     outgoing[...] = dot(dispatch.astype(BF16), ffn_ref[:, own].astype(BF16)).astype(BF16)
     sends = {}
-    steps = sorted(range(1, ep_count), key=lambda step: abs(2 * step - ep_count))
+    steps = range(1, ep_count)
     for step in steps:
         sends[step] = (
             pltpu.make_async_remote_copy(
@@ -281,7 +281,7 @@
     combine_high = combine.astype(BF16)
     combine_low = (combine - combine_high.astype(F32)).astype(BF16)
 
-    for step in reversed(steps):
+    for step in steps:
         sends[step].wait_recv()
         relays.append(
             pltpu.make_async_remote_copy(

time: 42.3 us -> 40 us (0.946)
  Pallas kernels: 40 us -> 37.7 us
    pallas_call x1, Pallas kernels: 30.5 us -> 28.2 us  [on_device(): pl.pallas_call(functools.partial(expert_kernel, cap), out_shape=jax.Shape...]
where the time goes in v3:
time: 40 us; the launch traced here: 39.8 us
  Pallas kernels  37.7 us (94%)
  local copies, waits for them, and re-layouts  1.42 us (4%)
  between operations  0.65 us (2%)
    pallas_call x1, Pallas kernels, on_device(): pl.pallas_call(functools.partial(expert_kernel, cap), out_shape=jax.Shape...  28.2 us
    pallas_call x1, Pallas kernels, on_device(): pl.pallas_call(functools.partial(mixer_kernel, names), out_shape=(jax.Sha...  9.54 us
    unnamed x1, local copies, waits for them, and re-layouts  1.42 us

profile of v3, /device:TPU:0, one launch (start us, length us, event | category | flops | bytes accessed | tf_op | source)
XLA Modules:
  0.0 39.8 jit_solution(15082356515751638145)
XLA Ops:
  0.6 9.5 %mixer.1 = (bf16[22,512]{1,0:T(8,128)(2,1)}, f32[22,8,64,128]{3,2,1,0:T(8,128)}) custom-call(bf16[22,2048]{1,0:T(8,128)(2,1)} %hidden_ref.1, bf16[2048]{0:T(1024)(128)(2,1)} %refs_1_.1, bf16[16,2048]{1,0:T(8,128)(2,1)} %bitcast.9, bf16[4,512]{1,0:T(4,128)(2,1)} %refs_3_.1, bf16[3,22,256]{2,1,0:T(8,128)(2,1)} %bitcast.10, bf16[2048,256]{1,0:T(8,128)(2,1)} %refs_5_.1, ...), custom_call_target="tpu_custom_call" | custom-call | tf_op jit(solution)/shard_map/mixer/pallas_call | solution.py:402
  10.2 28.2 %experts.1 = bf16[22,1024]{1,0:T(8,128)(2,1)} custom-call(bf16[22,512]{1,0:T(8,128)(2,1)} %get-tuple-element.4.mixed_ref, bf16[22,2048]{1,0:T(8,128)(2,1)} %hidden_ref.1, bf16[2048]{0:T(1024)(128)(2,1)} %gain_ref.1, bf16[2,2048]{1,0:T(2,128)(2,1)} %bitcast.12, bf16[16,2048]{1,0:T(8,128)(2,1)} %bitcast.8, s32[3,22]{1,0:T(4,128)} %bitcast.13, ...), custom_call_target="tpu_custom_call" | custom-call | tf_op jit(solution)/shard_map/experts/pallas_call | solution.py:422
  38.3 1.4 %copy.29 = bf16[22,1024]{1,0:T(8,128)(2,1)} copy(bf16[22,1024]{1,0:T(8,128)(2,1)} %experts.1) | data formatting | bytes 90112
